TPU v7x, 32 devices: a whole 2x2x4 slice. The times are simulated.
32 devices in a mesh: fs: 16 (over z, y, x), tp: 2 (over core).
Axes of the slice: x: 2, y: 2, z: 4, core: 2. Of those that a mesh axis runs over, the one named last changes fastest.
Arguments:
- saved_inputs: bfloat16 [12288, 2048], P('fs'), may hold values from -8 to 8
- input_cot: bfloat16 [12288, 2048], P('fs', 'tp'), may hold values from -0.0546875 to 0.0546875
- gate_cot: bfloat16 [12288, 2048], P('fs', 'tp'), may hold values from -0.0546875 to 0.0546875
- input_master: float32 [2048, 2048], P('fs', 'tp'), may hold values from -6 to 6
- gate_master: float32 [2048, 2048], P('fs', 'tp'), may hold values from -6 to 6
- input_factor: bfloat16 [2048, 256], P('fs'), may hold values from -2 to 2
- gate_factor: bfloat16 [2048, 256], P('fs'), may hold values from -2 to 2
- input_first: float32 [256, 2048], P('fs', 'tp'), may hold values from -6 to 6
- input_second: float32 [256, 2048], P('fs', 'tp'), may hold values from 0.2 to 17
- gate_first: float32 [256, 2048], P('fs', 'tp'), may hold values from -6 to 6
- gate_second: float32 [256, 2048], P('fs', 'tp'), may hold values from 0.2 to 17
Outputs:
- input_step: float32 [2048, 2048], P('fs', 'tp')
- gate_step: float32 [2048, 2048], P('fs', 'tp')
- input_first_new: float32 [256, 2048], P('fs', 'tp')
- input_second_new: float32 [256, 2048], P('fs', 'tp')
- gate_first_new: float32 [256, 2048], P('fs', 'tp')
- gate_second_new: float32 [256, 2048], P('fs', 'tp')
- input_copy: bfloat16 [2048, 2048], P(None, 'tp')
- gate_copy: bfloat16 [2048, 2048], P(None, 'tp')
All inputs are finite; a program needn't handle non-finite values.
Results may differ from a plain program's by a relative error of at most 0.0004.
Values may be sent and summed in bfloat16 or wider, within the bound.
A program may use at most 64 MiB of HBM per device.

v0:
```python
import jax
import jax.numpy as jnp
from jax import lax
from jax.sharding import PartitionSpec as P

D = 2048
W = 2048
first_decay = 0.9
second_decay = 0.9
ratio_floor = 1e-08
mean_floor = 1e-06
step_size = 0.05


def moments(low_rank, first, second):
    first_new = first_decay * first + (1.0 - first_decay) * low_rank
    second_new = second_decay * second + (1.0 - second_decay) * low_rank * low_rank
    ratio = first_new / (jnp.sqrt(second_new) + ratio_floor)
    return (first_new, second_new, ratio)


def local(
    saved_inputs,
    input_cot,
    gate_cot,
    input_master,
    gate_master,
    input_factor,
    gate_factor,
    input_first,
    input_second,
    gate_first,
    gate_second,
):
    col_width = input_cot.shape[1]
    contract = (((0,), (0,)), ((), ()))
    factor_in = input_factor.astype(jnp.float32)
    factor_gate = gate_factor.astype(jnp.float32)
    whole_in, whole_gate = (
        lax.all_gather(input_factor, "fs", axis=0, tiled=True),
        lax.all_gather(gate_factor, "fs", axis=0, tiled=True),
    )
    partial_in = lax.dot_general(
        saved_inputs, input_cot, contract, preferred_element_type=jnp.float32
    )
    partial_gate = lax.dot_general(
        saved_inputs, gate_cot, contract, preferred_element_type=jnp.float32
    )
    cols_in = whole_in.astype(jnp.float32)
    cols_gate = whole_gate.astype(jnp.float32)
    term_in = lax.dot_general(cols_in, partial_in, contract, precision=lax.Precision.HIGHEST)
    term_gate = lax.dot_general(cols_gate, partial_gate, contract, precision=lax.Precision.HIGHEST)
    summed = lax.psum_scatter(
        jnp.concatenate([term_in, term_gate], axis=1), "fs", scatter_dimension=0, tiled=True
    )
    low_in = summed[:, :col_width]
    low_gate = summed[:, col_width:]
    first_in, second_in, ratio_in = moments(low_in, input_first, input_second)
    first_gate, second_gate, ratio_gate = moments(low_gate, gate_first, gate_second)
    piece_in = lax.all_gather(ratio_in, "fs", axis=0, tiled=True)
    piece_gate = lax.all_gather(ratio_gate, "fs", axis=0, tiled=True)
    cols_in = factor_in
    cols_gate = factor_gate
    dir_in = jnp.dot(cols_in, piece_in, precision=lax.Precision.HIGHEST)
    dir_gate = jnp.dot(cols_gate, piece_gate, precision=lax.Precision.HIGHEST)
    square_in, square_gate = lax.psum(
        (jnp.sum(dir_in * dir_in), jnp.sum(dir_gate * dir_gate)), ("fs", "tp")
    )
    step_in = dir_in * lax.rsqrt(square_in / (D * W) + mean_floor)
    step_gate = dir_gate * lax.rsqrt(square_gate / (D * W) + mean_floor)
    local_in = (input_master - step_size * step_in).astype(jnp.bfloat16)
    local_gate = (gate_master - step_size * step_gate).astype(jnp.bfloat16)
    copy_in, copy_gate = (
        lax.all_gather(local_in, "fs", axis=0, tiled=True),
        lax.all_gather(local_gate, "fs", axis=0, tiled=True),
    )
    return (step_in, step_gate, first_in, second_in, first_gate, second_gate, copy_in, copy_gate)


def solution(mesh):
    return jax.shard_map(
        local,
        mesh=mesh,
        in_specs=(
            P("fs", None),
            P("fs", "tp"),
            P("fs", "tp"),
            P("fs", "tp"),
            P("fs", "tp"),
            P("fs", None),
            P("fs", None),
            P("fs", "tp"),
            P("fs", "tp"),
            P("fs", "tp"),
            P("fs", "tp"),
        ),
        out_specs=(
            P("fs", "tp"),
            P("fs", "tp"),
            P("fs", "tp"),
            P("fs", "tp"),
            P("fs", "tp"),
            P("fs", "tp"),
            P(None, "tp"),
            P(None, "tp"),
        ),
        check_vma=False,
    )
```

profile of v0, /device:TPU:0, one launch (start us, length us, event | category | flops | bytes accessed | tf_op | source)
XLA Modules:
  0.0 569.3 jit_solution(10387800890137530023)
XLA Ops:
  7.2 0.0 copy-start
  7.2 0.0 all-gather.7.cloned.1.call-start
  7.2 0.7 all-gather.7.cloned.1.call-update
  7.9 0.0 all-gather.9.cloned.1.call-start
  8.0 0.7 all-gather.9.cloned.1.call-update
  8.7 0.0 reduce-scatter.4.cloned.1.call-start
  8.7 0.3 copy-done
  9.1 0.0 copy-start.8
  9.1 7.2 %fusion.4 = f32[2048,1024]{1,0:T(8,128)} fusion(bf16[768,2048]{1,0:T(8,128)(2,1)S(1)} %copy-done, bf16[768,1024]{1,0:T(8,128)(2,1)} %param.12), kind=kOutput, calls=%fused_computation.17 | convolution fusion | flops 3221225472 | bytes 13107200 | tf_op jit(solution)/shard_map/dot_general | solution.py:43
  16.2 0.0 copy-done.8
  16.2 5.7 %fusion.5 = f32[2048,1024]{1,0:T(8,128)} fusion(bf16[768,2048]{1,0:T(8,128)(2,1)S(1)} %copy-done, bf16[768,1024]{1,0:T(8,128)(2,1)S(1)} %copy-done.8), kind=kOutput, calls=%fused_computation.18 | convolution fusion | flops 3221225472 | bytes 13107200 | tf_op jit(solution)/shard_map/dot_general | solution.py:46
  21.9 46.7 %all-gather.7.cloned.1.call-done = bf16[2048,256]{1,0:T(8,128)(2,1)} async-done(((bf16[128,256]{1,0:T(8,128)(2,1)}), bf16[2048,256]{1,0:T(8,128)(2,1)}) %all-gather.7.cloned.1.call-update) | async-done | bytes 1048592 | tf_op jit(solution)/shard_map/all_gather | solution.py:40
  68.6 11.2 %convolution_bitcast_fusion.1 = f32[256,1024]{0,1:T(8,128)} fusion(f32[2048,1024]{1,0:T(8,128)} %fusion.4, bf16[2048,256]{1,0:T(8,128)(2,1)} %all-gather.7.cloned.1.call-done), kind=kOutput, calls=%fused_computation.2 | convolution fusion | flops 6442450944 | bytes 10485760 | tf_op jit(solution)/shard_map/dot_general | solution.py:51
  79.8 45.5 %all-gather.9.cloned.1.call-done = bf16[2048,256]{1,0:T(8,128)(2,1)} async-done(((bf16[128,256]{1,0:T(8,128)(2,1)}), bf16[2048,256]{1,0:T(8,128)(2,1)}) %all-gather.9.cloned.1.call-update) | async-done | bytes 1048592 | tf_op jit(solution)/shard_map/all_gather | solution.py:41
  125.3 0.0 copy-start.1
  125.3 9.5 %convolution_bitcast_fusion = f32[256,1024]{0,1:T(8,128)S(1)} fusion(f32[2048,1024]{1,0:T(8,128)} %fusion.5, bf16[2048,256]{1,0:T(8,128)(2,1)} %all-gather.9.cloned.1.call-done), kind=kOutput, calls=%fused_computation.1 | convolution fusion | flops 6442450944 | bytes 10485760 | tf_op jit(solution)/shard_map/dot_general | solution.py:52
  134.8 0.0 copy-done.1
  134.8 1.5 pad_maximum_fusion
  136.2 0.0 copy-start.4
  136.2 0.0 copy-start.5
  136.2 0.0 copy-start.6
  136.2 0.0 copy-start.7
  136.2 0.0 copy-start.2
  136.3 2.9 copy.65
  139.2 0.0 copy-start.3
  139.2 0.0 reduce-scatter.4.cloned.1.call-update
  139.2 0.0 all-gather.13.cloned.1.call-start
  139.3 80.6 %reduce-scatter.4.cloned.1.call-done = f32[16,2048]{1,0:T(8,128)} async-done(((f32[256,2048]{1,0:T(8,128)}), f32[16,2048]{1,0:T(8,128)}) %reduce-scatter.4.cloned.1.call-update) | async-done | bytes 131088 | tf_op jit(solution)/shard_map/reduce_scatter | solution.py:53
  219.9 0.0 copy-done.4
  219.9 0.0 copy-done.5
  219.9 0.0 copy-done.6
  219.9 0.0 copy-done.7
  219.9 1.6 add_divide_fusion
  221.5 0.0 all-gather.13.cloned.1.call-update
  221.5 0.0 all-gather.11.cloned.1.call-start
  221.6 0.5 all-gather.11.cloned.1.call-update
  222.1 0.0 all-gather.15.cloned.1.call-start
  222.2 2.0 copy.59
  224.2 50.4 %all-gather.13.cloned.1.call-done = f32[256,1024]{1,0:T(8,128)} async-done(((f32[16,1024]{1,0:T(8,128)}), f32[256,1024]{1,0:T(8,128)}) %all-gather.13.cloned.1.call-update) | async-done | bytes 1048592 | tf_op jit(solution)/shard_map/all_gather | solution.py:61
  274.6 0.0 copy-done.2
  274.6 3.7 multiply_reduce_fusion
  278.3 53.4 %all-gather.11.cloned.1.call-done = f32[256,1024]{1,0:T(8,128)} async-done(((f32[16,1024]{1,0:T(8,128)}), f32[256,1024]{1,0:T(8,128)}) %all-gather.11.cloned.1.call-update) | async-done | bytes 1048592 | tf_op jit(solution)/shard_map/all_gather | solution.py:60
  331.7 0.0 copy-done.3
  331.7 3.6 multiply_reduce_fusion.1
  335.4 38.6 %all-reduce = (f32[]{:T(128)}, f32[]{:T(128)}) all-reduce(f32[]{:T(128)} %get-tuple-element.47, f32[]{:T(128)} %get-tuple-element.49), channel_id=1, replica_groups=mesh['fs'=16,'tp'=2] {'fs','tp'}, use_global_device_ids=true, to_apply=%region_2.0 | all-reduce | flops 2 | bytes 16 | tf_op jit(solution)/shard_map/psum | solution.py:66
  374.7 2.2 subtract_convert_fusion.1
  376.8 0.0 all-gather.15.cloned.1.call-update
  376.9 0.0 all-gather.17.cloned.1.call-start
  376.9 2.0 copy.60
  379.7 2.2 subtract_convert_fusion
  381.8 0.0 all-gather.17.cloned.1.call-update
  381.9 2.0 copy.61
  383.9 2.0 copy.62
  385.9 80.5 %all-gather.15.cloned.1.call-done = bf16[2048,1024]{0,1:T(8,128)(2,1)} async-done(((bf16[128,1024]{0,1:T(8,128)(2,1)}), bf16[2048,1024]{0,1:T(8,128)(2,1)}) %all-gather.15.cloned.1.call-update) | async-done | bytes 4194320 | tf_op jit(solution)/shard_map/all_gather | solution.py:74
  466.4 6.4 %copy.63 = bf16[2048,1024]{1,0:T(8,128)(2,1)} copy(bf16[2048,1024]{0,1:T(8,128)(2,1)} %all-gather.15.cloned.1.call-done) | data formatting | bytes 8388608
  472.8 83.2 %all-gather.17.cloned.1.call-done = bf16[2048,1024]{0,1:T(8,128)(2,1)} async-done(((bf16[128,1024]{0,1:T(8,128)(2,1)}), bf16[2048,1024]{0,1:T(8,128)(2,1)}) %all-gather.17.cloned.1.call-update) | async-done | bytes 4194320 | tf_op jit(solution)/shard_map/all_gather | solution.py:75
  556.0 6.4 %copy.64 = bf16[2048,1024]{1,0:T(8,128)(2,1)} copy(bf16[2048,1024]{0,1:T(8,128)(2,1)} %all-gather.17.cloned.1.call-done) | data formatting | bytes 8388608
Async XLA Ops:
  7.2 1.9 copy-start
  7.2 61.4 %all-gather.7.cloned.1.call-start = ((), (), s32[]{:S(2)}) async-start(), calls=%async_computation.1 | async-start | bytes 1114112 | tf_op jit(solution)/shard_map/all_gather | solution.py:40
  7.9 117.4 %all-gather.9.cloned.1.call-start = ((), (), s32[]{:S(2)}) async-start(), calls=%async_computation.2 | async-start | bytes 1114112 | tf_op jit(solution)/shard_map/all_gather | solution.py:41
  8.7 211.2 %reduce-scatter.4.cloned.1.call-start = ((), (), s32[]{:S(2)}) async-start(), calls=%async_computation.7 | async-start | bytes 2228224 | tf_op jit(solution)/shard_map/reduce_scatter | solution.py:53
  9.1 7.2 %copy-start.8 = (bf16[768,1024]{1,0:T(8,128)(2,1)S(1)}, bf16[768,1024]{1,0:T(8,128)(2,1)}, u32[]{:S(2)}) copy-start(bf16[768,1024]{1,0:T(8,128)(2,1)} %param.13) | copy-start | bytes 4718596
  125.3 9.5 %copy-start.1 = (f32[256,1024]{0,1:T(8,128)S(1)}, f32[256,1024]{0,1:T(8,128)}, u32[]{:S(2)}) copy-start(f32[256,1024]{0,1:T(8,128)} %convolution_bitcast_fusion.1) | copy-start | bytes 3145732
  136.2 83.6 %copy-start.4 = (f32[16,1024]{1,0:T(8,128)S(1)}, f32[16,1024]{1,0:T(8,128)}, u32[]{:S(2)}) copy-start(f32[16,1024]{1,0:T(8,128)} %param.21) | copy-start | bytes 196612
  136.2 83.6 %copy-start.5 = (f32[16,1024]{1,0:T(8,128)S(1)}, f32[16,1024]{1,0:T(8,128)}, u32[]{:S(2)}) copy-start(f32[16,1024]{1,0:T(8,128)} %param.20) | copy-start | bytes 196612
  136.2 83.6 %copy-start.6 = (f32[16,1024]{1,0:T(8,128)S(1)}, f32[16,1024]{1,0:T(8,128)}, u32[]{:S(2)}) copy-start(f32[16,1024]{1,0:T(8,128)} %param.19) | copy-start | bytes 196612
  136.2 83.6 %copy-start.7 = (f32[16,1024]{1,0:T(8,128)S(1)}, f32[16,1024]{1,0:T(8,128)}, u32[]{:S(2)}) copy-start(f32[16,1024]{1,0:T(8,128)} %param.18) | copy-start | bytes 196612
  136.2 138.3 %copy-start.2 = (bf16[128,256]{1,0:T(8,128)(2,1)S(1)}, bf16[128,256]{1,0:T(8,128)(2,1)}, u32[]{:S(2)}) copy-start(bf16[128,256]{1,0:T(8,128)(2,1)} %param.17) | copy-start | bytes 196612
  139.2 192.5 %copy-start.3 = (bf16[128,256]{1,0:T(8,128)(2,1)S(1)}, bf16[128,256]{1,0:T(8,128)(2,1)}, u32[]{:S(2)}) copy-start(bf16[128,256]{1,0:T(8,128)(2,1)} %param.16) | copy-start | bytes 196612
  139.2 135.4 %all-gather.13.cloned.1.call-start = ((), (), s32[]{:S(2)}) async-start(), calls=%async_computation.4 | async-start | bytes 1114112 | tf_op jit(solution)/shard_map/all_gather | solution.py:61
  221.5 110.2 %all-gather.11.cloned.1.call-start = ((), (), s32[]{:S(2)}) async-start(), calls=%async_computation.3 | async-start | bytes 1114112 | tf_op jit(solution)/shard_map/all_gather | solution.py:60
  222.1 244.3 %all-gather.15.cloned.1.call-start = ((), (), s32[]{:S(2)}) async-start(), calls=%async_computation.5 | async-start | bytes 4456448 | tf_op jit(solution)/shard_map/all_gather | solution.py:74
  376.9 179.2 %all-gather.17.cloned.1.call-start = ((), (), s32[]{:S(2)}) async-start(), calls=%async_computation.6 | async-start | bytes 4456448 | tf_op jit(solution)/shard_map/all_gather | solution.py:75
Sparse Core Ops, SparseCore 0:
  10.7 57.7 all-gather.6
  71.3 53.9 all-gather.8
  139.3 80.4 reduce-scatter.3
  223.0 51.4 all-gather.12
  277.8 53.9 all-gather.10
  377.0 89.3 all-gather.14
  469.1 86.8 all-gather.16
where the time goes:
time: 570 us; the launch traced here: 569 us
  waiting for transfers between devices  442 us (78%)
  matrix products  40.9 us (7%)
  blocking collectives  38.6 us (7%)
  local copies, waits for them, and re-layouts  24.2 us (4%)
  between operations  15.6 us (3%)
  other arithmetic  7.42 us (1%)
    all_gather x1, waiting for transfers between devices, local(): lax.all_gather(local_gate, 'fs', axis=0, tiled=True)  83.2 us
    reduce_scatter x1, waiting for transfers between devices, local(): lax.psum_scatter(jnp.concatenate([term_in, term_gate], axis=1), 'fs', sca...  80.6 us
    all_gather x1, waiting for transfers between devices, local(): lax.all_gather(local_in, 'fs', axis=0, tiled=True)  80.5 us
    all_gather x1, waiting for transfers between devices, local(): piece_in = lax.all_gather(ratio_in, 'fs', axis=0, tiled=True)  53.4 us
    all_gather x1, waiting for transfers between devices, local(): piece_gate = lax.all_gather(ratio_gate, 'fs', axis=0, tiled=True)  50.4 us
    all_gather x1, waiting for transfers between devices, local(): lax.all_gather(input_factor, 'fs', axis=0, tiled=True)  46.7 us
    all_gather x1, waiting for transfers between devices, local(): lax.all_gather(gate_factor, 'fs', axis=0, tiled=True)  45.5 us
    psum x1, blocking collectives, local(): lax.psum((jnp.sum(dir_in * dir_in), jnp.sum(dir_gate * dir_gate)), ('fs',...  38.6 us
  transfers between devices with their start and end apart: 7, of which 7 were waited for; matrix products, arithmetic and copies ran while one was open for 8% of the time, Pallas kernels for 0%

commit v1 on v0

--- a/solution.py
+++ b/solution.py
@@ -64,7 +64,7 @@
     dir_in = jnp.dot(cols_in, piece_in, precision=lax.Precision.HIGHEST)
     dir_gate = jnp.dot(cols_gate, piece_gate, precision=lax.Precision.HIGHEST)
     square_in, square_gate = lax.psum(
-        (jnp.sum(dir_in * dir_in), jnp.sum(dir_gate * dir_gate)), ("fs", "tp")
+        lax.psum((jnp.sum(dir_in * dir_in), jnp.sum(dir_gate * dir_gate)), "fs"), "tp"
     )
     step_in = dir_in * lax.rsqrt(square_in / (D * W) + mean_floor)
     step_gate = dir_gate * lax.rsqrt(square_gate / (D * W) + mean_floor)

time: 570 us -> 570 us (level)
    psum x1 -> x2, blocking collectives: 38.6 us -> 43.4 us  [the longest x1 40.3 us: local(): lax.psum((jnp.sum(dir_in * dir_in), jnp.sum(dir_gate * dir_gate)), 'fs')]
where the time goes in v1:
time: 570 us; the launch traced here: 569 us
  waiting for transfers between devices  437 us (77%)
  blocking collectives  43.4 us (8%)
  matrix products  40.8 us (7%)
  local copies, waits for them, and re-layouts  24.3 us (4%)
  between operations  15.6 us (3%)
  other arithmetic  7.46 us (1%)
    all_gather x1, waiting for transfers between devices, local(): lax.all_gather(local_gate, 'fs', axis=0, tiled=True)  83.2 us
    reduce_scatter x1, waiting for transfers between devices, local(): lax.psum_scatter(jnp.concatenate([term_in, term_gate], axis=1), 'fs', sca...  80.4 us
    all_gather x1, waiting for transfers between devices, local(): lax.all_gather(local_in, 'fs', axis=0, tiled=True)  75.6 us
    all_gather x1, waiting for transfers between devices, local(): piece_in = lax.all_gather(ratio_in, 'fs', axis=0, tiled=True)  53.5 us
    all_gather x1, waiting for transfers between devices, local(): piece_gate = lax.all_gather(ratio_gate, 'fs', axis=0, tiled=True)  50.6 us
    all_gather x1, waiting for transfers between devices, local(): lax.all_gather(input_factor, 'fs', axis=0, tiled=True)  46.7 us
    all_gather x1, waiting for transfers between devices, local(): lax.all_gather(gate_factor, 'fs', axis=0, tiled=True)  45.5 us
    psum x1, blocking collectives, local(): lax.psum((jnp.sum(dir_in * dir_in), jnp.sum(dir_gate * dir_gate)), 'fs')  40.3 us
  transfers between devices with their start and end apart: 7, of which 7 were waited for; matrix products, arithmetic and copies ran while one was open for 8% of the time, Pallas kernels for 0%

profile of v1, /device:TPU:0, one launch (start us, length us, event | category | flops | bytes accessed | tf_op | source)
XLA Modules:
  0.0 569.4 jit_solution(12057421192152946405)
XLA Ops:
  7.2 0.0 copy-start
  7.2 0.0 all-gather.7.cloned.1.call-start
  7.2 0.7 all-gather.7.cloned.1.call-update
  7.9 0.0 all-gather.9.cloned.1.call-start
  8.0 0.7 all-gather.9.cloned.1.call-update
  8.7 0.0 reduce-scatter.4.cloned.1.call-start
  8.7 0.3 copy-done
  9.1 0.0 copy-start.8
  9.1 7.2 %fusion.4 = f32[2048,1024]{1,0:T(8,128)} fusion(bf16[768,2048]{1,0:T(8,128)(2,1)S(1)} %copy-done, bf16[768,1024]{1,0:T(8,128)(2,1)} %param.12), kind=kOutput, calls=%fused_computation.17 | convolution fusion | flops 3221225472 | bytes 13107200 | tf_op jit(solution)/shard_map/dot_general | solution.py:43
  16.2 0.0 copy-done.8
  16.2 5.7 %fusion.5 = f32[2048,1024]{1,0:T(8,128)} fusion(bf16[768,2048]{1,0:T(8,128)(2,1)S(1)} %copy-done, bf16[768,1024]{1,0:T(8,128)(2,1)S(1)} %copy-done.8), kind=kOutput, calls=%fused_computation.18 | convolution fusion | flops 3221225472 | bytes 13107200 | tf_op jit(solution)/shard_map/dot_general | solution.py:46
  21.9 46.7 %all-gather.7.cloned.1.call-done = bf16[2048,256]{1,0:T(8,128)(2,1)} async-done(((bf16[128,256]{1,0:T(8,128)(2,1)}), bf16[2048,256]{1,0:T(8,128)(2,1)}) %all-gather.7.cloned.1.call-update) | async-done | bytes 1048592 | tf_op jit(solution)/shard_map/all_gather | solution.py:40
  68.6 11.2 %convolution_bitcast_fusion.1 = f32[256,1024]{0,1:T(8,128)} fusion(f32[2048,1024]{1,0:T(8,128)} %fusion.4, bf16[2048,256]{1,0:T(8,128)(2,1)} %all-gather.7.cloned.1.call-done), kind=kOutput, calls=%fused_computation.2 | convolution fusion | flops 6442450944 | bytes 10485760 | tf_op jit(solution)/shard_map/dot_general | solution.py:51
  79.8 45.5 %all-gather.9.cloned.1.call-done = bf16[2048,256]{1,0:T(8,128)(2,1)} async-done(((bf16[128,256]{1,0:T(8,128)(2,1)}), bf16[2048,256]{1,0:T(8,128)(2,1)}) %all-gather.9.cloned.1.call-update) | async-done | bytes 1048592 | tf_op jit(solution)/shard_map/all_gather | solution.py:41
  125.3 0.0 copy-start.1
  125.3 9.5 %convolution_bitcast_fusion = f32[256,1024]{0,1:T(8,128)S(1)} fusion(f32[2048,1024]{1,0:T(8,128)} %fusion.5, bf16[2048,256]{1,0:T(8,128)(2,1)} %all-gather.9.cloned.1.call-done), kind=kOutput, calls=%fused_computation.1 | convolution fusion | flops 6442450944 | bytes 10485760 | tf_op jit(solution)/shard_map/dot_general | solution.py:52
  134.8 0.0 copy-done.1
  134.8 1.5 pad_maximum_fusion
  136.2 0.0 copy-start.4
  136.2 0.0 copy-start.5
  136.2 0.0 copy-start.6
  136.2 0.0 copy-start.7
  136.2 0.0 copy-start.2
  136.3 2.9 copy.65
  139.2 0.0 copy-start.3
  139.2 0.0 reduce-scatter.4.cloned.1.call-update
  139.2 0.0 all-gather.13.cloned.1.call-start
  139.3 80.4 %reduce-scatter.4.cloned.1.call-done = f32[16,2048]{1,0:T(8,128)} async-done(((f32[256,2048]{1,0:T(8,128)}), f32[16,2048]{1,0:T(8,128)}) %reduce-scatter.4.cloned.1.call-update) | async-done | bytes 131088 | tf_op jit(solution)/shard_map/reduce_scatter | solution.py:53
  219.7 0.0 copy-done.4
  219.7 0.0 copy-done.5
  219.7 0.0 copy-done.6
  219.7 0.0 copy-done.7
  219.7 1.6 add_divide_fusion
  221.3 0.0 all-gather.13.cloned.1.call-update
  221.3 0.0 all-gather.11.cloned.1.call-start
  221.4 0.5 all-gather.11.cloned.1.call-update
  221.9 0.0 all-gather.15.cloned.1.call-start
  222.0 2.0 copy.59
  224.0 50.6 %all-gather.13.cloned.1.call-done = f32[256,1024]{1,0:T(8,128)} async-done(((f32[16,1024]{1,0:T(8,128)}), f32[256,1024]{1,0:T(8,128)}) %all-gather.13.cloned.1.call-update) | async-done | bytes 1048592 | tf_op jit(solution)/shard_map/all_gather | solution.py:61
  274.6 0.0 copy-done.2
  274.6 3.6 multiply_reduce_fusion
  278.3 53.5 %all-gather.11.cloned.1.call-done = f32[256,1024]{1,0:T(8,128)} async-done(((f32[16,1024]{1,0:T(8,128)}), f32[256,1024]{1,0:T(8,128)}) %all-gather.11.cloned.1.call-update) | async-done | bytes 1048592 | tf_op jit(solution)/shard_map/all_gather | solution.py:60
  331.8 0.0 copy-done.3
  331.8 3.6 multiply_reduce_fusion.1
  335.4 40.3 %all-reduce = (f32[]{:T(128)}, f32[]{:T(128)}) all-reduce(f32[]{:T(128)} %get-tuple-element.49, f32[]{:T(128)} %get-tuple-element.51), channel_id=1, replica_groups=mesh['fs'=16,'tp'=2] {'fs'}, use_global_device_ids=true, to_apply=%region_2.0 | all-reduce | flops 2 | bytes 16 | tf_op jit(solution)/shard_map/psum | solution.py:67
  375.7 3.2 all-reduce.1
  379.5 2.2 subtract_convert_fusion.1
  381.7 0.0 all-gather.15.cloned.1.call-update
  381.7 0.0 all-gather.17.cloned.1.call-start
  381.7 2.0 copy.60
  384.5 2.2 subtract_convert_fusion
  386.7 0.0 all-gather.17.cloned.1.call-update
  386.8 2.1 copy.61
  388.8 2.0 copy.62
  390.8 75.6 %all-gather.15.cloned.1.call-done = bf16[2048,1024]{0,1:T(8,128)(2,1)} async-done(((bf16[128,1024]{0,1:T(8,128)(2,1)}), bf16[2048,1024]{0,1:T(8,128)(2,1)}) %all-gather.15.cloned.1.call-update) | async-done | bytes 4194320 | tf_op jit(solution)/shard_map/all_gather | solution.py:74
  466.5 6.4 %copy.63 = bf16[2048,1024]{1,0:T(8,128)(2,1)} copy(bf16[2048,1024]{0,1:T(8,128)(2,1)} %all-gather.15.cloned.1.call-done) | data formatting | bytes 8388608
  472.9 83.2 %all-gather.17.cloned.1.call-done = bf16[2048,1024]{0,1:T(8,128)(2,1)} async-done(((bf16[128,1024]{0,1:T(8,128)(2,1)}), bf16[2048,1024]{0,1:T(8,128)(2,1)}) %all-gather.17.cloned.1.call-update) | async-done | bytes 4194320 | tf_op jit(solution)/shard_map/all_gather | solution.py:75
  556.1 6.4 %copy.64 = bf16[2048,1024]{1,0:T(8,128)(2,1)} copy(bf16[2048,1024]{0,1:T(8,128)(2,1)} %all-gather.17.cloned.1.call-done) | data formatting | bytes 8388608
Async XLA Ops:
  7.2 1.9 copy-start
  7.2 61.4 %all-gather.7.cloned.1.call-start = ((), (), s32[]{:S(2)}) async-start(), calls=%async_computation.1 | async-start | bytes 1114112 | tf_op jit(solution)/shard_map/all_gather | solution.py:40
  7.9 117.4 %all-gather.9.cloned.1.call-start = ((), (), s32[]{:S(2)}) async-start(), calls=%async_computation.2 | async-start | bytes 1114112 | tf_op jit(solution)/shard_map/all_gather | solution.py:41
  8.7 211.0 %reduce-scatter.4.cloned.1.call-start = ((), (), s32[]{:S(2)}) async-start(), calls=%async_computation.7 | async-start | bytes 2228224 | tf_op jit(solution)/shard_map/reduce_scatter | solution.py:53
  9.1 7.2 %copy-start.8 = (bf16[768,1024]{1,0:T(8,128)(2,1)S(1)}, bf16[768,1024]{1,0:T(8,128)(2,1)}, u32[]{:S(2)}) copy-start(bf16[768,1024]{1,0:T(8,128)(2,1)} %param.13) | copy-start | bytes 4718596
  125.3 9.5 %copy-start.1 = (f32[256,1024]{0,1:T(8,128)S(1)}, f32[256,1024]{0,1:T(8,128)}, u32[]{:S(2)}) copy-start(f32[256,1024]{0,1:T(8,128)} %convolution_bitcast_fusion.1) | copy-start | bytes 3145732
  136.2 83.4 %copy-start.4 = (f32[16,1024]{1,0:T(8,128)S(1)}, f32[16,1024]{1,0:T(8,128)}, u32[]{:S(2)}) copy-start(f32[16,1024]{1,0:T(8,128)} %param.21) | copy-start | bytes 196612
  136.2 83.4 %copy-start.5 = (f32[16,1024]{1,0:T(8,128)S(1)}, f32[16,1024]{1,0:T(8,128)}, u32[]{:S(2)}) copy-start(f32[16,1024]{1,0:T(8,128)} %param.20) | copy-start | bytes 196612
  136.2 83.4 %copy-start.6 = (f32[16,1024]{1,0:T(8,128)S(1)}, f32[16,1024]{1,0:T(8,128)}, u32[]{:S(2)}) copy-start(f32[16,1024]{1,0:T(8,128)} %param.19) | copy-start | bytes 196612
  136.2 83.4 %copy-start.7 = (f32[16,1024]{1,0:T(8,128)S(1)}, f32[16,1024]{1,0:T(8,128)}, u32[]{:S(2)}) copy-start(f32[16,1024]{1,0:T(8,128)} %param.18) | copy-start | bytes 196612
  136.2 138.4 %copy-start.2 = (bf16[128,256]{1,0:T(8,128)(2,1)S(1)}, bf16[128,256]{1,0:T(8,128)(2,1)}, u32[]{:S(2)}) copy-start(bf16[128,256]{1,0:T(8,128)(2,1)} %param.17) | copy-start | bytes 196612
  139.2 192.6 %copy-start.3 = (bf16[128,256]{1,0:T(8,128)(2,1)S(1)}, bf16[128,256]{1,0:T(8,128)(2,1)}, u32[]{:S(2)}) copy-start(bf16[128,256]{1,0:T(8,128)(2,1)} %param.16) | copy-start | bytes 196612
  139.2 135.4 %all-gather.13.cloned.1.call-start = ((), (), s32[]{:S(2)}) async-start(), calls=%async_computation.4 | async-start | bytes 1114112 | tf_op jit(solution)/shard_map/all_gather | solution.py:61
  221.3 110.4 %all-gather.11.cloned.1.call-start = ((), (), s32[]{:S(2)}) async-start(), calls=%async_computation.3 | async-start | bytes 1114112 | tf_op jit(solution)/shard_map/all_gather | solution.py:60
  221.9 244.6 %all-gather.15.cloned.1.call-start = ((), (), s32[]{:S(2)}) async-start(), calls=%async_computation.5 | async-start | bytes 4456448 | tf_op jit(solution)/shard_map/all_gather | solution.py:74
  381.7 174.4 %all-gather.17.cloned.1.call-start = ((), (), s32[]{:S(2)}) async-start(), calls=%async_computation.6 | async-start | bytes 4456448 | tf_op jit(solution)/shard_map/all_gather | solution.py:75
Sparse Core Ops, SparseCore 0:
  10.7 57.7 all-gather.6
  71.3 53.9 all-gather.8
  139.3 80.2 reduce-scatter.3
  222.9 51.7 all-gather.12
  277.8 53.9 all-gather.10
  381.8 84.6 all-gather.14
  469.2 86.8 all-gather.16
